TPU v7x, 32 devices: a whole 2x2x4 slice. The times are simulated.
32 devices in a mesh: sp: 8 (over z, y), tp: 4 (over x, core).
Axes of the slice: x: 2, y: 2, z: 4, core: 2. Of those that a mesh axis runs over, the one named last changes fastest.
Arguments:
- stream: bfloat16 [1024, 2048], P('sp', 'tp'), may hold values from -40 to 40
- queries: bfloat16 [1024, 1024], P('sp', 'tp'), may hold values from -6 to 6
- keys: bfloat16 [1024, 1024], P('sp', 'tp'), may hold values from -6 to 6
- values: bfloat16 [1024, 2048], P('sp', 'tp'), may hold values from -25 to 25
- out_gate: bfloat16 [1024, 2048], P('sp', 'tp'), may hold values from -8 to 8
- input_gate: float32 [1024, 8], P('sp', 'tp'), may hold values from -9 to 350
- forget_gate: float32 [1024, 8], P('sp', 'tp'), may hold values from -4 to 20
- head_gain: float32 [2048], P('tp'), may hold values from 0.1 to 1.9
- w_out: bfloat16 [2048, 2048], P('tp'), may hold values from -0.125 to 0.125
- ffn_gain: float32 [2048], replicated, may hold values from 0.1 to 1.9
- w_gate: bfloat16 [2048, 5632], P('sp', 'tp'), may hold values from -0.125 to 0.125
- w_up: bfloat16 [2048, 5632], P('sp', 'tp'), may hold values from -0.125 to 0.125
- w_down: bfloat16 [5632, 2048], P('tp', 'sp'), may hold values from -0.078125 to 0.078125
Outputs:
- mixed: bfloat16 [1024, 2048], P('sp', 'tp')
All inputs are finite; a program needn't handle non-finite values.
Results may differ from a plain program's by a relative error of at most 0.0095.
Values may be sent and summed in bfloat16 or wider, within the bound.
No kernel may reach another device: no remote copies, remote signals or barrier semaphores. Data moves between devices by JAX's collectives and lax.ppermute only.
A program may use at most 128 MiB of HBM per device.

v0:
```python
import jax
import jax.numpy as jnp
from jax import lax
from jax.sharding import PartitionSpec as P

D = 2048
DQK = 128
DV = 256
BLOCK = 64
VALS = 2048
precise = lax.Precision.HIGHEST
norm_eps = 1e-06
very_low = -1e30


def entering(value, axis, join, neutral):
    count, mine = (lax.axis_size(axis), lax.axis_index(axis))
    pieces = jax.tree.map(lambda part: lax.all_gather(part, axis), value)
    subtotal = jax.tree.map(
        lambda part, zero: jnp.full_like(part, 0) + jnp.asarray(zero, part.dtype), value, neutral
    )

    def step(position, subtotal):
        longer = join(subtotal, jax.tree.map(lambda part: part[position], pieces))
        return jax.tree.map(lambda new, old: jnp.where(position < mine, new, old), longer, subtotal)

    return lax.fori_loop(0, count - 1, step, subtotal)


def block_summary(key_blk, value_blk, input_blk, decay_sum):
    decay_total = decay_sum[..., -1]
    log_weight = decay_total[..., None] - decay_sum + input_blk
    weight_peak = jnp.max(log_weight, axis=-1)
    weights = jnp.exp(log_weight - weight_peak[..., None])
    state_mat = jnp.einsum(
        "...ld,...le->...de", weights[..., None] * key_blk, value_blk, precision=precise
    )
    state_vec = jnp.einsum("...l,...ld->...d", weights, key_blk, precision=precise)
    return (state_mat, state_vec, weight_peak, decay_total)


def combine(earlier, later):
    ceiling = jnp.maximum(later[3] + earlier[2], later[2])
    former = jnp.exp(later[3] + earlier[2] - ceiling)
    latter = jnp.exp(later[2] - ceiling)
    return (
        former[..., None, None] * earlier[0] + latter[..., None, None] * later[0],
        former[..., None] * earlier[1] + latter[..., None] * later[1],
        ceiling,
        earlier[3] + later[3],
    )


def block_output(
    query_blk, key_blk, value_blk, input_blk, decay_sum, state_mat, state_vec, state_peak
):
    block_len = query_blk.shape[-2]
    causal = jnp.tril(jnp.ones((block_len, block_len), jnp.bool_))
    log_pair = jnp.where(
        causal,
        decay_sum[..., :, None] - decay_sum[..., None, :] + input_blk[..., None, :],
        -jnp.inf,
    )
    log_carry = decay_sum + state_peak[..., None]
    row_peak = jnp.maximum(log_carry, jnp.max(log_pair, axis=-1))
    scores = jnp.einsum("...ld,...sd->...ls", query_blk, key_blk, precision=precise) * jnp.exp(
        log_pair - row_peak[..., None]
    )
    carried = jnp.exp(log_carry - row_peak)
    numer = jnp.einsum("...ls,...se->...le", scores, value_blk, precision=precise) + carried[
        ..., None
    ] * jnp.einsum("...ld,...de->...le", query_blk, state_mat, precision=precise)
    normer = jnp.sum(scores, axis=-1) + carried * jnp.einsum(
        "...ld,...d->...l", query_blk, state_vec, precision=precise
    )
    denom = jnp.maximum(jnp.abs(normer), jnp.exp(-row_peak))
    return numer / denom[..., None]


def local(
    stream,
    queries,
    keys,
    values,
    out_gate,
    input_gate,
    forget_gate,
    head_gain,
    w_out,
    ffn_gain,
    w_gate,
    w_up,
    w_down,
):
    gate_full, up_full, down_full = (
        lax.all_gather(w_gate, "sp", axis=0, tiled=True),
        lax.all_gather(w_up, "sp", axis=0, tiled=True),
        lax.all_gather(w_down, "sp", axis=1, tiled=True),
    )
    count_of_rows = stream.shape[0]
    head_count = input_gate.shape[1]
    blocks = count_of_rows // BLOCK

    def to_blocks(array, col_width):
        return (
            array.astype(jnp.float32)
            .reshape(blocks, BLOCK, head_count, col_width)
            .transpose(2, 0, 1, 3)
        )

    query_blk = to_blocks(queries, DQK) * DQK ** (-0.5)
    key_blk = to_blocks(keys, DQK)
    value_blk = to_blocks(values, DV)
    input_blk = input_gate.reshape(blocks, BLOCK, head_count).transpose(2, 0, 1)
    decay_sum = jnp.cumsum(
        jax.nn.log_sigmoid(forget_gate).reshape(blocks, BLOCK, head_count).transpose(2, 0, 1),
        axis=-1,
    )
    summary = block_summary(key_blk, value_blk, input_blk, decay_sum)
    identity = (
        jnp.zeros((head_count, DQK, DV), jnp.float32),
        jnp.zeros((head_count, DQK), jnp.float32),
        jnp.full((head_count,), very_low, jnp.float32),
        jnp.zeros((head_count,), jnp.float32),
    )

    def advance(carry, piece):
        return (combine(carry, piece), carry)

    local_total, prefix = lax.scan(
        advance, identity, jax.tree.map(lambda array: jnp.moveaxis(array, 1, 0), summary)
    )
    carry_in = entering(local_total, "sp", combine, identity)
    start = combine(
        jax.tree.map(lambda array: array[:, None], carry_in),
        jax.tree.map(lambda array: jnp.moveaxis(array, 0, 1), prefix),
    )
    mixed_heads = block_output(
        query_blk, key_blk, value_blk, input_blk, decay_sum, start[0], start[1], start[2]
    )
    head_rows = mixed_heads.transpose(1, 2, 0, 3).reshape(count_of_rows, head_count, DV)
    local_sq = jnp.sum(head_rows * head_rows, axis=(1, 2))
    total_sq = lax.psum(local_sq, "tp")
    row_scale = lax.rsqrt(total_sq / VALS + norm_eps)
    gated = (
        head_rows
        * row_scale[:, None, None]
        * head_gain.reshape(head_count, DV)
        * jax.nn.sigmoid(out_gate.astype(jnp.float32).reshape(count_of_rows, head_count, DV))
    )
    heads_out = gated.reshape(count_of_rows, head_count * DV).astype(jnp.bfloat16)
    partial_value = jnp.dot(heads_out, w_out, preferred_element_type=jnp.float32)
    col_width = stream.shape[1]
    col_start = lax.axis_index("tp") * col_width
    mixer_own = lax.psum_scatter(
        partial_value.astype(jnp.bfloat16), "tp", scatter_dimension=1, tiled=True
    ).astype(jnp.float32)
    resid_own = (stream.astype(jnp.float32) + mixer_own).astype(jnp.bfloat16)
    resid_f = resid_own.astype(jnp.float32)
    square_total = lax.psum(jnp.sum(resid_f * resid_f, axis=-1), "tp")
    gain_own = lax.dynamic_slice_in_dim(ffn_gain, col_start, col_width)
    normed_own = (resid_f * lax.rsqrt(square_total / D + norm_eps)[:, None] * gain_own).astype(
        jnp.bfloat16
    )
    normed = lax.all_gather(normed_own, "tp", axis=1, tiled=True)
    gate_act = jnp.dot(normed, gate_full, preferred_element_type=jnp.float32)
    up_act = jnp.dot(normed, up_full, preferred_element_type=jnp.float32)
    hidden = (jax.nn.silu(gate_act) * up_act).astype(jnp.bfloat16)
    term = jnp.dot(hidden, down_full, preferred_element_type=jnp.float32)
    down_own = lax.psum_scatter(
        term.astype(jnp.bfloat16), "tp", scatter_dimension=1, tiled=True
    ).astype(jnp.float32)
    return (resid_own.astype(jnp.float32) + down_own).astype(jnp.bfloat16)


def solution(mesh):
    in_specs = (
        P("sp", "tp"),
        P("sp", "tp"),
        P("sp", "tp"),
        P("sp", "tp"),
        P("sp", "tp"),
        P("sp", "tp"),
        P("sp", "tp"),
        P("tp"),
        P("tp", None),
        P(),
        P("sp", "tp"),
        P("sp", "tp"),
        P("tp", "sp"),
    )
    out_specs = P("sp", "tp")
    return jax.shard_map(local, mesh=mesh, in_specs=in_specs, out_specs=out_specs, check_vma=False)
```

profile of v0, /device:TPU:0, one launch (start us, length us, event | category | flops | bytes accessed | tf_op | source)
XLA Modules:
  0.0 422.1 jit_solution(10034435100602329406)
XLA Ops:
  6.6 0.8 fusion.59
  8.2 0.8 reshape.66
  9.2 0.9 reshape.64
  10.0 0.9 reshape.67
  11.8 2.2 while.43
  16.5 23.2 %all-reduce.2 = (f32[16]{0:T(128)S(1)}, f32[16]{0:T(128)S(1)}) all-reduce(f32[16]{0:T(128)S(1)} %dynamic-update-slice, f32[16]{0:T(128)S(1)} %dynamic-update-slice.1), channel_id=2, replica_groups=mesh['sp'=8,'tp'=4] {'sp'}, use_global_device_ids=true, to_apply=%add | all-reduce | flops 32 | bytes 256
  40.0 16.7 %all-gather.4 = f32[8,2,128]{2,1,0:T(2,128)S(1)} all-gather(f32[1,2,128]{2,1,0:T(2,128)S(1)} %bitcast.218), channel_id=5, replica_groups=mesh['sp'=8,'tp'=4] {'sp'}, dimensions={0}, use_global_device_ids=true | all-gather | bytes 9216 | tf_op jit(solution)/shard_map/all_gather | solution.py:18
  56.8 10.0 %all-gather.16.cloned.1.call-done = f32[16,128,256]{2,1,0:T(8,128)} async-done(((f32[2,128,256]{2,1,0:T(8,128)}), f32[16,128,256]{2,1,0:T(8,128)}) %all-gather.16.cloned.1.call-update) | async-done | bytes 2097168 | tf_op jit(solution)/shard_map/all_gather | solution.py:18
  66.8 8.3 %while.44 = (s32[]{:T(128)}, f32[2,128,256]{2,1,0:T(8,128)S(1)}, f32[2,128]{1,0:T(2,128)S(1)}, f32[2]{0:T(128)S(1)}, s32[]{:T(128)}, /*index=5*/f32[8,2]{1,0:T(8...) while((s32[]{:T(128)}, f32[2,128,256]{2,1,0:T(8,128)S(1)}, ...), condition=%wide.region_5.6_spmd.clone, body=%wide.region_4.5_spmd.clone.sunk | while | flops 328978 | bytes 789757 | solution.py:27
  66.9 1.1 fusion.87
  68.1 1.1 fusion.87
  69.2 1.1 fusion.87
  70.4 1.1 fusion.87
  71.6 1.1 fusion.87
  72.8 1.1 fusion.87
  74.0 1.1 fusion.87
  76.5 1.7 multiply_reduce_fusion
  78.5 5.6 %psum.14 = f32[128]{0:T(128)S(1)} all-reduce(f32[128]{0:T(128)S(1)} %reduce_sum.34), channel_id=1, replica_groups=mesh['sp'=8,'tp'=4] {'tp'}, use_global_device_ids=true, to_apply=%region_9.10 | all-reduce | flops 128 | bytes 1024 | tf_op jit(solution)/shard_map/psum | solution.py:143
  84.2 1.3 convolution_convert_fusion
  87.5 0.8 dynamic_slice.46
  88.2 17.9 %reduce-scatter.3.cloned.1.call-done = bf16[128,512]{1,0:T(8,128)(2,1)} async-done(((bf16[128,2048]{1,0:T(8,128)(2,1)}), bf16[128,512]{1,0:T(8,128)(2,1)}) %reduce-scatter.3.cloned.1.call-update) | async-done | bytes 131088 | tf_op jit(solution)/shard_map/reduce_scatter | solution.py:155
  106.1 1.0 fusion.25
  107.1 5.8 %psum.15 = f32[128]{0:T(128)S(1)} all-reduce(f32[128]{0:T(128)S(1)} %fusion.25), channel_id=1, replica_groups=mesh['sp'=8,'tp'=4] {'tp'}, use_global_device_ids=true, to_apply=%region_12.13 | all-reduce | flops 128 | bytes 1024 | tf_op jit(solution)/shard_map/psum | solution.py:160
  112.9 1.0 fusion.27
  113.9 6.9 %all_gather.44 = bf16[128,2048]{1,0:T(8,128)(2,1)S(1)} all-gather(bf16[128,512]{1,0:T(8,128)(2,1)S(1)} %fusion.27), channel_id=1, replica_groups=mesh['sp'=8,'tp'=4] {'tp'}, dimensions={1}, use_global_device_ids=true | all-gather | bytes 655360 | tf_op jit(solution)/shard_map/all_gather | solution.py:165
  120.8 79.9 %all-gather.10.cloned.1.call-done = bf16[2048,1408]{1,0:T(8,128)(2,1)} async-done(((bf16[256,1408]{1,0:T(8,128)(2,1)}), bf16[2048,1408]{1,0:T(8,128)(2,1)}) %all-gather.10.cloned.1.call-update) | async-done | bytes 5767184 | tf_op jit(solution)/shard_map/all_gather | solution.py:96
  200.7 4.5 %fusion.68 = f32[128,1408]{1,0:T(8,128)} fusion(bf16[128,2048]{1,0:T(8,128)(2,1)S(1)} %all_gather.44, bf16[2048,1408]{1,0:T(8,128)(2,1)} %all-gather.10.cloned.1.call-done), kind=kOutput, calls=%fused_computation.119 | convolution fusion | flops 738197504 | bytes 7012352 | tf_op jit(solution)/shard_map/dot_general | solution.py:166
  205.2 88.0 %all-gather.12.cloned.1.call-done = bf16[2048,1408]{1,0:T(8,128)(2,1)} async-done(((bf16[256,1408]{1,0:T(8,128)(2,1)}), bf16[2048,1408]{1,0:T(8,128)(2,1)}) %all-gather.12.cloned.1.call-update) | async-done | bytes 5767184 | tf_op jit(solution)/shard_map/all_gather | solution.py:97
  293.2 93.2 %all-gather.14.cloned.1.call-done = bf16[1408,2048]{1,0:T(8,128)(2,1)} async-done(((bf16[1408,256]{1,0:T(8,128)(2,1)}), bf16[1408,2048]{1,0:T(8,128)(2,1)}) %all-gather.14.cloned.1.call-update) | async-done | bytes 5767184 | tf_op jit(solution)/shard_map/all_gather | solution.py:98
  386.5 7.2 %convolution_convert_fusion.1 = bf16[128,2048]{1,0:T(8,128)(2,1)} fusion(bf16[1408,2048]{1,0:T(8,128)(2,1)} %all-gather.14.cloned.1.call-done, bf16[128,2048]{1,0:T(8,128)(2,1)S(1)} %all_gather.44, bf16[2048,1408]{1,0:T(8,128)(2,1)} %all-gather.12.cloned.1.call-done, f32[128,1408]{1,0:T(8,128)} %fusion.68), kind=kOutput, calls=%fused_computation.40 | convolution fusion | flops 1477738496 | bytes 13303808 | tf_op jit(solution)/shard_map/dot_general | solution.py:169
  393.7 20.0 %reduce-scatter.5.cloned.1.call-done = bf16[128,512]{1,0:T(8,128)(2,1)} async-done(((bf16[128,2048]{1,0:T(8,128)(2,1)}), bf16[128,512]{1,0:T(8,128)(2,1)}) %reduce-scatter.5.cloned.1.call-update) | async-done | bytes 131088 | tf_op jit(solution)/shard_map/reduce_scatter | solution.py:170
  413.7 1.6 fusion.28
  (115 shorter events, 10.5 us)
Async XLA Ops:
  6.5 77.6 %copy-start = (bf16[512,2048]{1,0:T(8,128)(2,1)S(1)}, bf16[512,2048]{1,0:T(8,128)(2,1)}, u32[]{:S(2)}) copy-start(bf16[512,2048]{1,0:T(8,128)(2,1)} %param.25) | copy-start | bytes 6291460
  6.5 8.3 %copy-start.7 = (u32[32]{0:T(128)S(1)}, u32[32]{0:T(128)}, u32[]{:S(2)}) copy-start(u32[32]{0:T(128)} %constant.93) | copy-start | bytes 388
  6.5 33.4 %copy-start.4 = (bf16[128,256]{1,0:T(8,128)(2,1)S(1)}, bf16[128,256]{1,0:T(8,128)(2,1)}, u32[]{:S(2)}) copy-start(bf16[128,256]{1,0:T(8,128)(2,1)} %param.18) | copy-start | bytes 196612
  6.5 60.3 %all-gather.16.cloned.1.call-start = ((), (), s32[]{:S(2)}) async-start(), calls=%async_computation.7 | async-start | bytes 2359296 | tf_op jit(solution)/shard_map/all_gather | solution.py:18
  14.0 0.7 copy-start.1
  14.0 70.2 %copy-start.5 = (bf16[128,512]{1,0:T(8,128)(2,1)S(1)}, bf16[128,512]{1,0:T(8,128)(2,1)}, u32[]{:S(2)}) copy-start(bf16[128,512]{1,0:T(8,128)(2,1)} %param.21) | copy-start | bytes 393220
  14.0 70.1 %copy-start.6 = (f32[512]{0:T(512)S(1)}, f32[512]{0:T(512)}, u32[]{:S(2)}) copy-start(f32[512]{0:T(512)} %param.24) | copy-start | bytes 6148
  14.7 91.4 %reduce-scatter.3.cloned.1.call-start = ((), (), s32[]{:S(2)}) async-start(), calls=%async_computation.2 | async-start | bytes 655360 | tf_op jit(solution)/shard_map/reduce_scatter | solution.py:155
  75.1 31.0 %copy-start.2 = (bf16[128,512]{1,0:T(8,128)(2,1)S(1)}, bf16[128,512]{1,0:T(8,128)(2,1)}, u32[]{:S(2)}) copy-start(bf16[128,512]{1,0:T(8,128)(2,1)} %param.17) | copy-start | bytes 393220
  85.5 115.2 %all-gather.10.cloned.1.call-start = ((), (), s32[]{:S(2)}) async-start(), calls=%async_computation.3 | async-start | bytes 6488064 | tf_op jit(solution)/shard_map/all_gather | solution.py:96
  86.2 207.0 %all-gather.12.cloned.1.call-start = ((), (), s32[]{:S(2)}) async-start(), calls=%async_computation.4 | async-start | bytes 6488064 | tf_op jit(solution)/shard_map/all_gather | solution.py:97
  86.8 299.6 %all-gather.14.cloned.1.call-start = ((), (), s32[]{:S(2)}) async-start(), calls=%async_computation.5 | async-start | bytes 6488064 | tf_op jit(solution)/shard_map/all_gather | solution.py:98
  87.4 326.3 %reduce-scatter.5.cloned.1.call-start = ((), (), s32[]{:S(2)}) async-start(), calls=%async_computation.6 | async-start | bytes 655360 | tf_op jit(solution)/shard_map/reduce_scatter | solution.py:170
  205.2 208.5 %copy-start.3 = (bf16[128,512]{1,0:T(8,128)(2,1)S(1)}, bf16[128,512]{1,0:T(8,128)(2,1)}, u32[]{:S(2)}) copy-start(bf16[128,512]{1,0:T(8,128)(2,1)} %reduce-scatter.3.cloned.1.call-done) | copy-start | bytes 393220
Sparse Core Ops, SparseCore 0:
  14.9 51.9 all-gather.15
  85.6 20.4 reduce-scatter.2
  108.3 92.3 all-gather.9
  202.7 90.4 all-gather.11
  295.1 91.2 all-gather.13
  393.8 19.7 reduce-scatter.4
where the time goes:
time: 423 us; the launch traced here: 422 us
  waiting for transfers between devices  311 us (74%)
  blocking collectives  58.2 us (14%)
  matrix products  16.3 us (4%)
  other arithmetic  15.8 us (4%)
  between operations  14.4 us (3%)
  local copies, waits for them, and re-layouts  6.37 us (2%)
    all_gather x1, waiting for transfers between devices, local(): lax.all_gather(w_down, 'sp', axis=1, tiled=True)  93.2 us
    all_gather x1, waiting for transfers between devices, local(): lax.all_gather(w_up, 'sp', axis=0, tiled=True)  88 us
    all_gather x1, waiting for transfers between devices, local(): lax.all_gather(w_gate, 'sp', axis=0, tiled=True)  79.9 us
    unnamed x1, blocking collectives  23.2 us
    reduce_scatter x1, waiting for transfers between devices, local(): lax.psum_scatter(term.astype(jnp.bfloat16), 'tp', scatter_dimension=1, ti...  20 us
    reduce_scatter x1, waiting for transfers between devices, local(): lax.psum_scatter(partial_value.astype(jnp.bfloat16), 'tp', scatter_dimens...  17.9 us
    all_gather x1, blocking collectives, entering(): pieces = jax.tree.map(lambda part: lax.all_gather(part, axis), value)  16.7 us
    all_gather x1, waiting for transfers between devices, entering(): pieces = jax.tree.map(lambda part: lax.all_gather(part, axis), value)  10 us
  transfers between devices with their start and end apart: 6, of which 6 were waited for; matrix products, arithmetic and copies ran while one was open for 2% of the time, Pallas kernels for 0%

commit v1 on v0

--- a/solution.py
+++ b/solution.py
@@ -1,3 +1,4 @@
+import functools
 import jax
 import jax.numpy as jnp
 from jax import lax
@@ -11,6 +12,22 @@
 precise = lax.Precision.HIGHEST
 norm_eps = 1e-06
 very_low = -1e30
+
+
+def map_the_body(m, at_axis):
+    num = lax.psum(1, axis_name="sp")
+    frames = [m]
+    for w in tuple(range(1, num)):
+        inter = lax.ppermute(
+            frames[w - 1], axis_name="sp", perm=[(c, (c - 1) % num) for c in range(num)]
+        )
+        frames.append(inter)
+    parts_out = jnp.concatenate(frames, axis=at_axis)
+    e_next = jnp.roll(parts_out, lax.axis_index("sp") * m.shape[at_axis], axis=at_axis)
+    return e_next
+
+
+process_notes = functools.partial(map_the_body, at_axis=0)
 
 
 def entering(value, axis, join, neutral):
@@ -93,7 +110,7 @@
     w_down,
 ):
     gate_full, up_full, down_full = (
-        lax.all_gather(w_gate, "sp", axis=0, tiled=True),
+        process_notes(w_gate),
         lax.all_gather(w_up, "sp", axis=0, tiled=True),
         lax.all_gather(w_down, "sp", axis=1, tiled=True),
     )

time: 423 us -> 424 us (level)
  waiting for transfers between devices: 311 us -> 218 us
  local copies, waits for them, and re-layouts: 6.37 us -> 42 us
  starting transfers between devices: 0.2 us -> 33.1 us
  other arithmetic: 15.8 us -> 35.8 us
    ppermute x0 -> x7, waiting for transfers between devices: none -> 138 us  [map_the_body(): lax.ppermute(frames[w - 1], axis_name='sp', perm=[(c, (c - 1) % num) for...]
    all_gather x1, waiting for transfers between devices: 88 us -> 0.01 us  [local(): lax.all_gather(w_up, 'sp', axis=0, tiled=True)]
    all_gather x1 -> x0, waiting for transfers between devices: 79.9 us -> none  [local(): lax.all_gather(w_gate, 'sp', axis=0, tiled=True)]
    all_gather x1, waiting for transfers between devices: 93.2 us -> 51.8 us  [local(): lax.all_gather(w_down, 'sp', axis=1, tiled=True)]
    ppermute x0 -> x7, starting transfers between devices: none -> 33 us  [map_the_body(): lax.ppermute(frames[w - 1], axis_name='sp', perm=[(c, (c - 1) % num) for...]
    unnamed x24 -> x43, local copies, waits for them, and re-layouts: 1.95 us -> 28.7 us
    reduce_scatter x1, waiting for transfers between devices: 17.9 us -> 0.01 us  [local(): lax.psum_scatter(partial_value.astype(jnp.bfloat16), 'tp', scatter_dimens...]
    select_n x21, other arithmetic: 8.15 us -> 16.9 us  [step(): jnp.where(position < mine, new, old)]
  transfers between devices with their start and end apart: 6 -> 12, of which waited for: 6 -> 10; matrix products, arithmetic and copies ran while one was open for 2% -> 9% of each run, Pallas kernels for 0% -> 0%
where the time goes in v1:
time: 424 us; the launch traced here: 422 us
  waiting for transfers between devices  218 us (51%)
  blocking collectives  59.3 us (14%)
  local copies, waits for them, and re-layouts  42 us (10%)
  other arithmetic  35.8 us (8%)
  starting transfers between devices  33.1 us (8%)
  matrix products  19.4 us (5%)
  between operations  14 us (3%)
    ppermute x7, waiting for transfers between devices, map_the_body(): lax.ppermute(frames[w - 1], axis_name='sp', perm=[(c, (c - 1) % num) for...  138 us
    all_gather x1, waiting for transfers between devices, local(): lax.all_gather(w_down, 'sp', axis=1, tiled=True)  51.8 us
    ppermute x7, starting transfers between devices, map_the_body(): lax.ppermute(frames[w - 1], axis_name='sp', perm=[(c, (c - 1) % num) for...  33 us
    unnamed x43, local copies, waits for them, and re-layouts  28.7 us
    unnamed x1, blocking collectives  23.2 us
    reduce_scatter x1, waiting for transfers between devices, local(): lax.psum_scatter(term.astype(jnp.bfloat16), 'tp', scatter_dimension=1, ti...  20 us
    select_n x21, other arithmetic, step(): jnp.where(position < mine, new, old)  16.9 us
    all_gather x1, blocking collectives, entering(): pieces = jax.tree.map(lambda part: lax.all_gather(part, axis), value)  16.6 us
  transfers between devices with their start and end apart: 12, of which 10 were waited for; matrix products, arithmetic and copies ran while one was open for 9% of the time, Pallas kernels for 0%

profile of v1, /device:TPU:0, one launch (start us, length us, event | category | flops | bytes accessed | tf_op | source)
XLA Modules:
  0.0 422.1 jit_solution(7951234977871233525)
XLA Ops:
  11.8 8.1 %while.43 = (s32[]{:T(128)}, f32[2,128,256]{2,1,0:T(8,128)S(1)}, f32[2,128]{1,0:T(2,128)S(1)}, f32[2]{0:T(128)S(1)}, f32[2]{0:T(128)S(1)}, /*index=5*/f32[2,2,12...) while((s32[]{:T(128)}, f32[2,128,256]{2,1,0:T(8,128)S(1)}, ...), condition=%wide.region_3.4_spmd.clone, body=%wide.region_2.3_spmd.clone.sunk | while | flops 328979 | bytes 1317212 | solution.py:147
  23.0 23.2 %all-reduce.2 = (f32[16]{0:T(128)S(1)}, f32[16]{0:T(128)S(1)}) all-reduce(f32[16]{0:T(128)S(1)} %dynamic-update-slice, f32[16]{0:T(128)S(1)} %dynamic-update-slice.1), channel_id=2, replica_groups=mesh['sp'=8,'tp'=4] {'sp'}, use_global_device_ids=true, to_apply=%add | all-reduce | flops 32 | bytes 256
  48.5 16.6 %all-gather.4 = f32[8,2,128]{2,1,0:T(2,128)S(1)} all-gather(f32[1,2,128]{2,1,0:T(2,128)S(1)} %bitcast.217), channel_id=5, replica_groups=mesh['sp'=8,'tp'=4] {'sp'}, dimensions={0}, use_global_device_ids=true | all-gather | bytes 9216 | tf_op jit(solution)/shard_map/all_gather | solution.py:35
  65.3 7.4 %all-gather.13.cloned.1.call-done = f32[16,128,256]{2,1,0:T(8,128)} async-done(((f32[2,128,256]{2,1,0:T(8,128)}), f32[16,128,256]{2,1,0:T(8,128)}) %all-gather.13.cloned.1.call-update) | async-done | bytes 2097168 | tf_op jit(solution)/shard_map/all_gather | solution.py:35
  72.7 21.7 %while.44 = (s32[]{:T(128)}, f32[2,128,256]{2,1,0:T(8,128)S(1)}, f32[2,128]{1,0:T(2,128)S(1)}, f32[2]{0:T(128)}, s32[]{:T(128)}, /*index=5*/f32[8,2]{1,0:T(8,128...) while((s32[]{:T(128)}, f32[2,128,256]{2,1,0:T(8,128)S(1)}, ...), condition=%wide.region_5.6_spmd.clone, body=%wide.region_4.5_spmd.clone.sunk | while | flops 328978 | bytes 789757 | solution.py:44
  105.0 5.6 %psum.14 = f32[128]{0:T(128)S(1)} all-reduce(f32[128]{0:T(128)S(1)} %reduce_sum.34), channel_id=1, replica_groups=mesh['sp'=8,'tp'=4] {'tp'}, use_global_device_ids=true, to_apply=%region_9.10 | all-reduce | flops 128 | bytes 1024 | tf_op jit(solution)/shard_map/psum | solution.py:160
  110.7 2.2 convolution_convert_fusion
  114.3 2.3 collective-permute-start
  116.6 15.6 %collective-permute-done = bf16[256,1408]{1,0:T(8,128)(2,1)S(1)} collective-permute-done((bf16[256,1408]{1,0:T(8,128)(2,1)S(1)}, bf16[256,1408]{1,0:T(8,128)(2,1)S(1)}, u32[]{:S(2)}, u32[]{:S(2)}) %collective-permute-start) | collective-permute-done | bytes 720928 | tf_op jit(solution)/shard_map/ppermute | solution.py:21
  132.2 4.6 %collective-permute-start.1 = (bf16[256,1408]{1,0:T(8,128)(2,1)S(1)}, bf16[256,1408]{1,0:T(8,128)(2,1)S(1)}, u32[]{:S(2)}, u32[]{:S(2)}) collective-permute-start(bf16[256,1408]{1,0:T(8,128)(2,1)S(1)} %collective-permute-done), channel_id=1, source_target_pairs={{0,28},{4,0},{8,4},{12,8},{16,12},{20,16},{24,20},{28,24},{1,29},{... | collective-permute-start | bytes 2162696 | tf_op jit(solution)/shard_map/ppermute | solution.py:21
  136.9 22.9 %collective-permute-done.1 = bf16[256,1408]{1,0:T(8,128)(2,1)S(1)} collective-permute-done((bf16[256,1408]{1,0:T(8,128)(2,1)S(1)}, bf16[256,1408]{1,0:T(8,128)(2,1)S(1)}, u32[]{:S(2)}, u32[]{:S(2)}) %collective-permute-start.1) | collective-permute-done | bytes 720928 | tf_op jit(solution)/shard_map/ppermute | solution.py:21
  160.7 5.2 %collective-permute-start.2 = (bf16[256,1408]{1,0:T(8,128)(2,1)S(1)}, bf16[256,1408]{1,0:T(8,128)(2,1)}, u32[]{:S(2)}, u32[]{:S(2)}) collective-permute-start(bf16[256,1408]{1,0:T(8,128)(2,1)S(1)} %collective-permute-done.1), channel_id=1, source_target_pairs={{0,28},{4,0},{8,4},{12,8},{16,12},{20,16},{24,20},{28,24},{1,29},{... | collective-permute-start | bytes 2162696 | tf_op jit(solution)/shard_map/ppermute | solution.py:21
  165.9 23.9 %collective-permute-done.2 = bf16[256,1408]{1,0:T(8,128)(2,1)} collective-permute-done((bf16[256,1408]{1,0:T(8,128)(2,1)S(1)}, bf16[256,1408]{1,0:T(8,128)(2,1)}, u32[]{:S(2)}, u32[]{:S(2)}) %collective-permute-start.2) | collective-permute-done | bytes 720928 | tf_op jit(solution)/shard_map/ppermute | solution.py:21
  189.7 5.3 %collective-permute-start.3 = (bf16[256,1408]{1,0:T(8,128)(2,1)}, bf16[256,1408]{1,0:T(8,128)(2,1)}, u32[]{:S(2)}, u32[]{:S(2)}) collective-permute-start(bf16[256,1408]{1,0:T(8,128)(2,1)} %collective-permute-done.2), channel_id=1, source_target_pairs={{0,28},{4,0},{8,4},{12,8},{16,12},{20,16},{24,20},{28,24},{1,29},{... | collective-permute-start | bytes 2162696 | tf_op jit(solution)/shard_map/ppermute | solution.py:21
  195.8 29.4 %collective-permute-done.3 = bf16[256,1408]{1,0:T(8,128)(2,1)} collective-permute-done((bf16[256,1408]{1,0:T(8,128)(2,1)}, bf16[256,1408]{1,0:T(8,128)(2,1)}, u32[]{:S(2)}, u32[]{:S(2)}) %collective-permute-start.3) | collective-permute-done | bytes 720928 | tf_op jit(solution)/shard_map/ppermute | solution.py:21
  225.2 5.2 %collective-permute-start.4 = (bf16[256,1408]{1,0:T(8,128)(2,1)}, bf16[256,1408]{1,0:T(8,128)(2,1)S(1)}, u32[]{:S(2)}, u32[]{:S(2)}) collective-permute-start(bf16[256,1408]{1,0:T(8,128)(2,1)} %collective-permute-done.3), channel_id=1, source_target_pairs={{0,28},{4,0},{8,4},{12,8},{16,12},{20,16},{24,20},{28,24},{1,29},{... | collective-permute-start | bytes 2162696 | tf_op jit(solution)/shard_map/ppermute | solution.py:21
  234.3 26.6 %collective-permute-done.4 = bf16[256,1408]{1,0:T(8,128)(2,1)S(1)} collective-permute-done((bf16[256,1408]{1,0:T(8,128)(2,1)}, bf16[256,1408]{1,0:T(8,128)(2,1)S(1)}, u32[]{:S(2)}, u32[]{:S(2)}) %collective-permute-start.4) | collective-permute-done | bytes 720928 | tf_op jit(solution)/shard_map/ppermute | solution.py:21
  260.9 5.1 %collective-permute-start.5 = (bf16[256,1408]{1,0:T(8,128)(2,1)S(1)}, bf16[256,1408]{1,0:T(8,128)(2,1)}, u32[]{:S(2)}, u32[]{:S(2)}) collective-permute-start(bf16[256,1408]{1,0:T(8,128)(2,1)S(1)} %collective-permute-done.4), channel_id=1, source_target_pairs={{0,28},{4,0},{8,4},{12,8},{16,12},{20,16},{24,20},{28,24},{1,29},{... | collective-permute-start | bytes 2162696 | tf_op jit(solution)/shard_map/ppermute | solution.py:21
  270.9 14.6 %collective-permute-done.5 = bf16[256,1408]{1,0:T(8,128)(2,1)} collective-permute-done((bf16[256,1408]{1,0:T(8,128)(2,1)S(1)}, bf16[256,1408]{1,0:T(8,128)(2,1)}, u32[]{:S(2)}, u32[]{:S(2)}) %collective-permute-start.5) | collective-permute-done | bytes 720928 | tf_op jit(solution)/shard_map/ppermute | solution.py:21
  285.6 5.3 %collective-permute-start.6 = (bf16[256,1408]{1,0:T(8,128)(2,1)}, bf16[256,1408]{1,0:T(8,128)(2,1)}, u32[]{:S(2)}, u32[]{:S(2)}) collective-permute-start(bf16[256,1408]{1,0:T(8,128)(2,1)} %collective-permute-done.5), channel_id=1, source_target_pairs={{0,28},{4,0},{8,4},{12,8},{16,12},{20,16},{24,20},{28,24},{1,29},{... | collective-permute-start | bytes 2162696 | tf_op jit(solution)/shard_map/ppermute | solution.py:21
  290.9 2.1 constant_dynamic-update-slice_fusion.10
  294.0 6.1 %psum.15 = f32[128]{0:T(128)S(1)} all-reduce(f32[128]{0:T(128)S(1)} %fusion.30), channel_id=1, replica_groups=mesh['sp'=8,'tp'=4] {'tp'}, use_global_device_ids=true, to_apply=%region_12.13 | all-reduce | flops 128 | bytes 1024 | tf_op jit(solution)/shard_map/psum | solution.py:177
  301.1 7.8 %all_gather.41 = bf16[128,2048]{1,0:T(8,128)(2,1)} all-gather(bf16[128,512]{1,0:T(8,128)(2,1)S(1)} %fusion.32), channel_id=1, replica_groups=mesh['sp'=8,'tp'=4] {'tp'}, dimensions={1}, use_global_device_ids=true | all-gather | bytes 655360 | tf_op jit(solution)/shard_map/all_gather | solution.py:182
  308.9 4.9 %collective-permute-done.6 = bf16[256,1408]{1,0:T(8,128)(2,1)} collective-permute-done((bf16[256,1408]{1,0:T(8,128)(2,1)}, bf16[256,1408]{1,0:T(8,128)(2,1)}, u32[]{:S(2)}, u32[]{:S(2)}) %collective-permute-start.6) | collective-permute-done | bytes 720928 | tf_op jit(solution)/shard_map/ppermute | solution.py:21
  319.8 2.1 constant_dynamic-update-slice_fusion.5
  321.9 2.1 constant_dynamic-update-slice_fusion.4
  326.0 2.1 constant_dynamic-update-slice_fusion.2
  328.1 2.1 constant_dynamic-update-slice_fusion.1
  330.2 4.7 %fusion.75 = f32[128,1408]{1,0:T(8,128)} fusion(bf16[128,2048]{1,0:T(8,128)(2,1)} %all_gather.41, bf16[2048,1408]{1,0:T(8,128)(2,1)} %all-gather.9.cloned.1.call-done), kind=kOutput, calls=%fused_computation.137 | convolution fusion | flops 738197504 | bytes 7012352 | tf_op jit(solution)/shard_map/dot_general | solution.py:184
  334.8 51.8 %all-gather.11.cloned.1.call-done = bf16[1408,2048]{1,0:T(8,128)(2,1)} async-done(((bf16[1408,256]{1,0:T(8,128)(2,1)}), bf16[1408,2048]{1,0:T(8,128)(2,1)}) %all-gather.11.cloned.1.call-update) | async-done | bytes 5767184 | tf_op jit(solution)/shard_map/all_gather | solution.py:115
  386.7 7.2 %convolution_convert_fusion.1 = bf16[128,2048]{1,0:T(8,128)(2,1)} fusion(bf16[1408,2048]{1,0:T(8,128)(2,1)} %all-gather.11.cloned.1.call-done, f32[128,1408]{1,0:T(8,128)} %fusion.75, bf16[128,2048]{1,0:T(8,128)(2,1)S(1)} %copy-done.5, bf16[4096,1408]{1,0:T(8,128)(2,1)} %constant_dynamic-update-slice_fusion.1, s32[]{:T(128)S(6)} %select_n.87), kind=kOutput, calls=%fused_computation.40 | convolution fusion | flops 1477738496 | bytes 13303812 | tf_op jit(solution)/shard_map/dot_general | solution.py:186
  393.9 20.0 %reduce-scatter.5.cloned.1.call-done = bf16[128,512]{1,0:T(8,128)(2,1)} async-done(((bf16[128,2048]{1,0:T(8,128)(2,1)}), bf16[128,512]{1,0:T(8,128)(2,1)}) %reduce-scatter.5.cloned.1.call-update) | async-done | bytes 131088 | tf_op jit(solution)/shard_map/reduce_scatter | solution.py:187
  (146 shorter events, 74.1 us)
Async XLA Ops:
  6.5 104.1 %copy-start = (bf16[512,2048]{1,0:T(8,128)(2,1)S(1)}, bf16[512,2048]{1,0:T(8,128)(2,1)}, u32[]{:S(2)}) copy-start(bf16[512,2048]{1,0:T(8,128)(2,1)} %param.25) | copy-start | bytes 6291460
  6.5 66.1 %all-gather.13.cloned.1.call-start = ((), (), s32[]{:S(2)}) async-start(), calls=%async_computation.6 | async-start | bytes 2359296 | tf_op jit(solution)/shard_map/all_gather | solution.py:35
  19.9 0.7 copy-start.1
  19.9 94.4 %copy-start.2 = (bf16[256,1408]{1,0:T(8,128)(2,1)S(1)}, bf16[256,1408]{1,0:T(8,128)(2,1)}, u32[]{:S(2)}) copy-start(bf16[256,1408]{1,0:T(8,128)(2,1)} %param.27) | copy-start | bytes 2162692
  20.6 272.3 %reduce-scatter.3.cloned.1.call-start = ((), (), s32[]{:S(2)}) async-start(), calls=%async_computation.2 | async-start | bytes 655360 | tf_op jit(solution)/shard_map/reduce_scatter | solution.py:172
  65.1 7.5 %copy-start.8 = (pred[64,64]{0,1:T(8,128)(4,1)}, pred[64,64]{0,1:T(8,128)(4,1)S(1)}, u32[]{:S(2)}) copy-start(pred[64,64]{0,1:T(8,128)(4,1)S(1)} %iota_compare_fusion) | copy-start | bytes 12292
  96.4 4.7 %copy-start.9 = (f32[2,2]{0,1:T(2,128)}, f32[2,2]{0,1:T(2,128)S(1)}, u32[]{:S(2)}) copy-start(f32[2,2]{0,1:T(2,128)S(1)} %fusion.65) | copy-start | bytes 52
  112.9 217.3 %all-gather.9.cloned.1.call-start = ((), (), s32[]{:S(2)}) async-start(), calls=%async_computation.3 | async-start | bytes 6488064 | tf_op jit(solution)/shard_map/all_gather | solution.py:114
  113.7 273.0 %all-gather.11.cloned.1.call-start = ((), (), s32[]{:S(2)}) async-start(), calls=%async_computation.4 | async-start | bytes 6488064 | tf_op jit(solution)/shard_map/all_gather | solution.py:115
  114.2 299.7 %reduce-scatter.5.cloned.1.call-start = ((), (), s32[]{:S(2)}) async-start(), calls=%async_computation.5 | async-start | bytes 655360 | tf_op jit(solution)/shard_map/reduce_scatter | solution.py:187
  114.3 18.0 %collective-permute-start = (bf16[256,1408]{1,0:T(8,128)(2,1)S(1)}, bf16[256,1408]{1,0:T(8,128)(2,1)S(1)}, u32[]{:S(2)}, u32[]{:S(2)}) collective-permute-start(bf16[256,1408]{1,0:T(8,128)(2,1)S(1)} %copy-done.2), channel_id=1, source_target_pairs={{0,28},{4,0},{8,4},{12,8},{16,12},{20,16},{24,20},{28,24},{1,29},{... | collective-permute-start | bytes 2162696 | tf_op jit(solution)/shard_map/ppermute | solution.py:21
  132.2 27.5 %collective-permute-start.1 = (bf16[256,1408]{1,0:T(8,128)(2,1)S(1)}, bf16[256,1408]{1,0:T(8,128)(2,1)S(1)}, u32[]{:S(2)}, u32[]{:S(2)}) collective-permute-start(bf16[256,1408]{1,0:T(8,128)(2,1)S(1)} %collective-permute-done), channel_id=1, source_target_pairs={{0,28},{4,0},{8,4},{12,8},{16,12},{20,16},{24,20},{28,24},{1,29},{... | collective-permute-start | bytes 2162696 | tf_op jit(solution)/shard_map/ppermute | solution.py:21
  159.8 0.9 copy-start.3
  160.7 29.0 %collective-permute-start.2 = (bf16[256,1408]{1,0:T(8,128)(2,1)S(1)}, bf16[256,1408]{1,0:T(8,128)(2,1)}, u32[]{:S(2)}, u32[]{:S(2)}) collective-permute-start(bf16[256,1408]{1,0:T(8,128)(2,1)S(1)} %collective-permute-done.1), channel_id=1, source_target_pairs={{0,28},{4,0},{8,4},{12,8},{16,12},{20,16},{24,20},{28,24},{1,29},{... | collective-permute-start | bytes 2162696 | tf_op jit(solution)/shard_map/ppermute | solution.py:21
  189.7 35.5 %collective-permute-start.3 = (bf16[256,1408]{1,0:T(8,128)(2,1)}, bf16[256,1408]{1,0:T(8,128)(2,1)}, u32[]{:S(2)}, u32[]{:S(2)}) collective-permute-start(bf16[256,1408]{1,0:T(8,128)(2,1)} %collective-permute-done.2), channel_id=1, source_target_pairs={{0,28},{4,0},{8,4},{12,8},{16,12},{20,16},{24,20},{28,24},{1,29},{... | collective-permute-start | bytes 2162696 | tf_op jit(solution)/shard_map/ppermute | solution.py:21
  225.2 35.7 %collective-permute-start.4 = (bf16[256,1408]{1,0:T(8,128)(2,1)}, bf16[256,1408]{1,0:T(8,128)(2,1)S(1)}, u32[]{:S(2)}, u32[]{:S(2)}) collective-permute-start(bf16[256,1408]{1,0:T(8,128)(2,1)} %collective-permute-done.3), channel_id=1, source_target_pairs={{0,28},{4,0},{8,4},{12,8},{16,12},{20,16},{24,20},{28,24},{1,29},{... | collective-permute-start | bytes 2162696 | tf_op jit(solution)/shard_map/ppermute | solution.py:21
  260.9 9.1 %copy-start.4 = (bf16[256,1408]{1,0:T(8,128)(2,1)}, bf16[256,1408]{1,0:T(8,128)(2,1)S(1)}, u32[]{:S(2)}) copy-start(bf16[256,1408]{1,0:T(8,128)(2,1)S(1)} %collective-permute-done.4) | copy-start | bytes 2162692
  260.9 24.7 %collective-permute-start.5 = (bf16[256,1408]{1,0:T(8,128)(2,1)S(1)}, bf16[256,1408]{1,0:T(8,128)(2,1)}, u32[]{:S(2)}, u32[]{:S(2)}) collective-permute-start(bf16[256,1408]{1,0:T(8,128)(2,1)S(1)} %collective-permute-done.4), channel_id=1, source_target_pairs={{0,28},{4,0},{8,4},{12,8},{16,12},{20,16},{24,20},{28,24},{1,29},{... | collective-permute-start | bytes 2162696 | tf_op jit(solution)/shard_map/ppermute | solution.py:21
  285.6 28.3 %collective-permute-start.6 = (bf16[256,1408]{1,0:T(8,128)(2,1)}, bf16[256,1408]{1,0:T(8,128)(2,1)}, u32[]{:S(2)}, u32[]{:S(2)}) collective-permute-start(bf16[256,1408]{1,0:T(8,128)(2,1)} %collective-permute-done.5), channel_id=1, source_target_pairs={{0,28},{4,0},{8,4},{12,8},{16,12},{20,16},{24,20},{28,24},{1,29},{... | collective-permute-start | bytes 2162696 | tf_op jit(solution)/shard_map/ppermute | solution.py:21
  316.8 69.9 %copy-start.5 = (bf16[128,2048]{1,0:T(8,128)(2,1)S(1)}, bf16[128,2048]{1,0:T(8,128)(2,1)}, u32[]{:S(2)}) copy-start(bf16[128,2048]{1,0:T(8,128)(2,1)} %all_gather.41) | copy-start | bytes 1572868
  328.1 85.8 %copy-start.6 = (bf16[128,512]{1,0:T(8,128)(2,1)S(1)}, bf16[128,512]{1,0:T(8,128)(2,1)}, u32[]{:S(2)}) copy-start(bf16[128,512]{1,0:T(8,128)(2,1)} %param.17) | copy-start | bytes 393220
  328.1 85.8 %copy-start.7 = (bf16[128,512]{1,0:T(8,128)(2,1)S(1)}, bf16[128,512]{1,0:T(8,128)(2,1)}, u32[]{:S(2)}) copy-start(bf16[128,512]{1,0:T(8,128)(2,1)} %reduce-scatter.3.cloned.1.call-done) | copy-start | bytes 393220
Sparse Core Ops, SparseCore 0:
  20.7 51.9 all-gather.12
  113.0 20.5 reduce-scatter.2
  135.8 144.3 all-gather.8
  282.1 104.5 all-gather.10
  394.1 19.7 reduce-scatter.4
